TPU v7x, 32 devices: a whole 2x2x4 slice. The times are simulated.
32 devices in a mesh: ep: 8 (over z, x), tp: 4 (over y, core).
Axes of the slice: x: 2, y: 2, z: 4, core: 2. Of those that a mesh axis runs over, the one named last changes fastest.
Arguments:
- tokens: bfloat16 [128, 4096], P('ep'), may hold values from -6 to 6
- norm_gain: float32 [4096], replicated, may hold values from 0.1 to 1.9
- query_weight: bfloat16 [4096, 2048], P('ep', 'tp'), may hold values from -0.09375 to 0.09375
- key_weight: bfloat16 [4096, 256], P('ep', 'tp'), may hold values from -0.09375 to 0.09375
- value_weight: bfloat16 [4096, 256], P('ep', 'tp'), may hold values from -0.09375 to 0.09375
- forget_weight: bfloat16 [4096, 32], P('ep', 'tp'), may hold values from -0.09375 to 0.09375
- forget_bias: float32 [32], P('tp'), may hold values from -1 to 2
- kv_cache: bfloat16 [128, 1024, 4, 128], P('ep', None, 'tp'), may hold values from -256 to 256, as said below
- log_gates: float32 [128, 1024, 32], P('ep', None, 'tp'), may hold values from -258 to 0
- lengths: int32 [128], P('ep'), may hold values from 128 to 1024, as said below
- out_weight: bfloat16 [2048, 4096], P('tp', 'ep'), may hold values from -0.125 to 0.125
- mix_gain: float32 [4096], replicated, may hold values from 0.1 to 1.9
- expert_gate: bfloat16 [8, 4096, 1024], P('ep', None, 'tp'), may hold values from -0.09375 to 0.09375
- expert_up: bfloat16 [8, 4096, 1024], P('ep', None, 'tp'), may hold values from -0.09375 to 0.09375
- expert_down: bfloat16 [8, 1024, 4096], P('ep', 'tp'), may hold values from -0.1875 to 0.1875
- routes: int32 [128, 4], P('ep'), may hold values from 0 to 7, all different within a row; in each aligned block of 16 rows (0 to 15, 16 to 31, ...) at most 16 rows name the same one
- route_weights: float32 [128, 4], P('ep'), may hold values from 0.2 to 1
- dense_gate: bfloat16 [4096, 4096], P(None, 'ep'), may hold values from -0.09375 to 0.09375
- dense_up: bfloat16 [4096, 4096], P(None, 'ep'), may hold values from -0.09375 to 0.09375
- dense_down: bfloat16 [4096, 4096], P('ep', 'tp'), may hold values from -0.09375 to 0.09375
- gate_vector: float32 [4096], replicated, may hold values from -0.09375 to 0.09375
Outputs:
- layer_out: bfloat16 [128, 4096], P('ep', 'tp')
Inputs may be any that keep to these rules, and one draw needn't show every extreme that they name: `kv_cache`: keys and values of the cached positions. `lengths`: some sequence uses all 1024 cached positions in every draw. A sequence's 4 experts differ. Among the routes of the 16 sequences of one index of ep no expert appears more than 16 times, and in every draw some expert appears exactly 16 times there; every expert is chosen somewhere.
All inputs are finite; a program needn't handle non-finite values.
Results may differ from a plain program's by a relative error of at most 0.012.
The roundings to bfloat16 on the way count: a program that leaves them out, or rounds other values in their place, can miss the bound.
Values may be sent and summed in bfloat16 or wider, within the bound.
No kernel may reach another device: no remote copies, remote signals or barrier semaphores. Data moves between devices by JAX's collectives and lax.ppermute only.
A program may use at most 128 MiB of HBM per device.

v0:
```python
import jax
import jax.numpy as jnp
from jax import lax
from jax.sharding import PartitionSpec as P

EPS = 1e-06


def rms_scaled(matrix, gains):
    values = matrix.astype(jnp.float32)
    return values * lax.rsqrt(jnp.mean(values * values, axis=-1, keepdims=True) + EPS) * gains


def attend_local(queries, key_new, value_new, forget, kv_cache, log_gates, lengths):
    seqs_here, cache_len, kv_count, double_width = kv_cache.shape
    head_width = double_width // 2
    group_size = queries.shape[1] // (kv_count * head_width)
    queries = queries.reshape(seqs_here, kv_count, group_size, head_width)
    key_new = key_new.reshape(seqs_here, kv_count, head_width)
    value_new = value_new.reshape(seqs_here, kv_count, head_width)
    cached_keys = kv_cache[..., :head_width]
    cached_values = kv_cache[..., head_width:]
    score_scale = head_width ** (-0.5)
    current_position = jnp.arange(cache_len, dtype=jnp.int32)
    is_last = (current_position[None, :] == lengths[:, None] - 1)[:, :, None]
    last_gate = jnp.sum(jnp.where(is_last, log_gates, 0.0), axis=1)
    newest = last_gate + forget
    gate_bias = newest[:, None, :] - log_gates
    gate_bias = gate_bias.reshape(seqs_here, cache_len, kv_count, group_size).transpose(0, 2, 3, 1)
    past_scores = (
        jnp.einsum("skgd,slkd->skgl", queries, cached_keys, preferred_element_type=jnp.float32)
        * score_scale
        + gate_bias
    )
    is_valid = (current_position[None, :] < lengths[:, None])[:, None, None, :]
    past_scores = jnp.where(is_valid, past_scores, -jnp.inf)
    own_score = (
        jnp.einsum("skgd,skd->skg", queries, key_new, preferred_element_type=jnp.float32)
        * score_scale
    )
    highest = jnp.maximum(jnp.max(past_scores, axis=-1), own_score)
    past_exp = jnp.exp(past_scores - highest[..., None])
    own_exp = jnp.exp(own_score - highest)
    totals = jnp.sum(past_exp, axis=-1) + own_exp
    past_weights = (past_exp / totals[..., None]).astype(jnp.bfloat16)
    own_weights = (own_exp / totals).astype(jnp.bfloat16)
    mixed_values = jnp.einsum(
        "skgl,slkd->skgd", past_weights, cached_values, preferred_element_type=jnp.float32
    )
    mixed_values = (
        mixed_values
        + own_weights.astype(jnp.float32)[..., None] * value_new.astype(jnp.float32)[:, :, None, :]
    )
    return mixed_values.astype(jnp.bfloat16).reshape(seqs_here, kv_count * group_size * head_width)


def shards(
    tokens,
    norm_gain,
    query_weight,
    key_weight,
    value_weight,
    forget_weight,
    forget_bias,
    kv_cache,
    log_gates,
    lengths,
    out_weight,
    mix_gain,
    expert_gate,
    expert_up,
    expert_down,
    routes,
    route_weights,
    dense_gate,
    dense_up,
    dense_down,
    gate_vector,
):
    seq_count = tokens.shape[0]
    normed = rms_scaled(tokens, norm_gain).astype(jnp.bfloat16)
    query_cols = query_weight.shape[1]
    key_cols = key_weight.shape[1]
    columns = lax.all_to_all(normed, "ep", split_axis=1, concat_axis=0, tiled=True)
    row_block = columns
    projected = lax.psum_scatter(
        jnp.concatenate(
            [
                jnp.dot(row_block, matrix, preferred_element_type=jnp.float32)
                for matrix in (query_weight, key_weight, value_weight, forget_weight)
            ],
            axis=1,
        ),
        "ep",
        scatter_dimension=0,
        tiled=True,
    )
    queries = projected[:, :query_cols].astype(jnp.bfloat16)
    key_new = projected[:, query_cols : query_cols + key_cols].astype(jnp.bfloat16)
    value_new = projected[:, query_cols + key_cols : query_cols + 2 * key_cols].astype(jnp.bfloat16)
    forget = jax.nn.log_sigmoid(projected[:, query_cols + 2 * key_cols :] + forget_bias)
    attended = attend_local(queries, key_new, value_new, forget, kv_cache, log_gates, lengths)
    column_terms = jnp.dot(
        lax.all_gather(attended, "ep", axis=0, tiled=True),
        out_weight,
        preferred_element_type=jnp.float32,
    )
    column_total = lax.psum(column_terms, "tp")
    summed = lax.all_to_all(column_total, "ep", split_axis=0, concat_axis=1, tiled=True)
    mixed = (tokens.astype(jnp.float32) + summed).astype(jnp.bfloat16)
    second = rms_scaled(mixed, mix_gain).astype(jnp.bfloat16)
    gate_value = jax.nn.sigmoid(
        jnp.dot(second.astype(jnp.float32), gate_vector, precision=lax.Precision.HIGHEST)
    )
    experts = lax.axis_size("ep")
    top_count = routes.shape[1]
    capacity = max(2, 2 * seq_count * top_count // experts)
    flat_routes = routes.reshape(-1)
    one_hot = (flat_routes[:, None] == jnp.arange(experts, dtype=jnp.int32)[None, :]).astype(
        jnp.int32
    )
    earlier = jnp.sum((jnp.cumsum(one_hot, axis=0) - one_hot) * one_hot, axis=1)
    slot_index = (flat_routes * capacity + earlier).reshape(seq_count, top_count)
    slot_ids = jnp.arange(experts * capacity, dtype=jnp.int32)
    dispatch_map = jnp.any(slot_index[None, :, :] == slot_ids[:, None, None], axis=2).astype(
        jnp.bfloat16
    )
    outgoing = jnp.dot(dispatch_map, second, preferred_element_type=jnp.float32).astype(
        jnp.bfloat16
    )
    outgoing = outgoing.reshape(experts, capacity, second.shape[1])
    received = lax.all_to_all(outgoing, "ep", split_axis=0, concat_axis=0, tiled=True)
    sources, items, model_width = received.shape
    flat_rows = received.reshape(sources * items, model_width)
    gate_pre = jnp.dot(flat_rows, expert_gate[0], preferred_element_type=jnp.float32)
    up_pre = jnp.dot(flat_rows, expert_up[0], preferred_element_type=jnp.float32)
    hidden = (jax.nn.silu(gate_pre) * up_pre).astype(jnp.bfloat16)
    partial_rows = jnp.dot(hidden, expert_down[0], preferred_element_type=jnp.float32)
    reduced = lax.psum_scatter(partial_rows, "tp", scatter_dimension=1, tiled=True)
    replies = reduced.astype(jnp.bfloat16).reshape(sources, items, reduced.shape[1])
    returned = lax.all_to_all(replies, "ep", split_axis=0, concat_axis=0, tiled=True)
    quarter_cols = returned.shape[2]
    picked = returned.reshape(experts * capacity, quarter_cols)[slot_index.reshape(-1)]
    routed = jnp.sum(
        picked.astype(jnp.float32).reshape(seq_count, top_count, quarter_cols)
        * route_weights[:, :, None],
        axis=1,
    )
    tp_index = lax.axis_index("tp")
    piece = lax.all_gather(second, "ep", axis=0, tiled=True)
    dense_hidden = (
        jax.nn.silu(jnp.dot(piece, dense_gate, preferred_element_type=jnp.float32))
        * jnp.dot(piece, dense_up, preferred_element_type=jnp.float32)
    ).astype(jnp.bfloat16)
    row_block = dense_hidden
    dense_out = lax.psum_scatter(
        jnp.dot(row_block, dense_down, preferred_element_type=jnp.float32),
        "ep",
        scatter_dimension=0,
        tiled=True,
    )
    residual = lax.dynamic_slice_in_dim(mixed, tp_index * quarter_cols, quarter_cols, 1).astype(
        jnp.float32
    )
    return (residual + routed + gate_value[:, None] * dense_out).astype(jnp.bfloat16)


def solution(mesh):
    return jax.shard_map(
        shards,
        mesh=mesh,
        in_specs=(
            P("ep", None),
            P(),
            P("ep", "tp"),
            P("ep", "tp"),
            P("ep", "tp"),
            P("ep", "tp"),
            P("tp"),
            P("ep", None, "tp", None),
            P("ep", None, "tp"),
            P("ep"),
            P("tp", "ep"),
            P(),
            P("ep", None, "tp"),
            P("ep", None, "tp"),
            P("ep", "tp", None),
            P("ep", None),
            P("ep", None),
            P(None, "ep"),
            P(None, "ep"),
            P("ep", "tp"),
            P(),
        ),
        out_specs=P("ep", "tp"),
        check_vma=False,
    )
```

profile of v0, /device:TPU:0, one launch (start us, length us, event | category | flops | bytes accessed | tf_op | source)
XLA Modules:
  0.0 333.0 jit_solution(12179301577359732236)
XLA Ops:
  6.6 1.2 fusion.48
  7.8 1.0 fusion.50
  8.9 14.4 %all_to_all.48 = bf16[16,8,512]{2,0,1:T(8,128)(2,1)S(1)} all-to-all(bf16[16,8,512]{2,0,1:T(8,128)(2,1)S(1)} %bitcast.121), channel_id=1, replica_groups=mesh['ep'=8,'tp'=4] {'ep'}, dimensions={1} | all-to-all | bytes 262144 | tf_op jit(solution)/shard_map/all_to_all | solution.py:84
  23.3 0.8 fusion.84
  24.1 1.0 fusion.83
  25.2 1.0 fusion.82
  26.2 1.3 fusion.81
  27.5 0.9 pad_maximum_fusion
  29.4 59.1 %reduce-scatter.4.cloned.1.call-done = f32[16,648]{1,0:T(8,128)} async-done(((f32[128,648]{1,0:T(8,128)}), f32[16,648]{1,0:T(8,128)}) %reduce-scatter.4.cloned.1.call-update) | async-done | bytes 41488 | tf_op jit(solution)/shard_map/reduce_scatter | solution.py:86
  89.6 0.9 fusion.69
  90.5 3.7 %fusion.80 = (f32[16,8]{1,0:T(8,128)S(1)}, f32[16,1,8,1024]{3,2,0,1:T(8,128)S(1)}) fusion(f32[16,1024,8]{1,2,0:T(8,128)S(1)} %copy-done.3, f32[16,8]{1,0:T(8,128)S(1)} %fusion.69, bf16[16,8,64]{2,1,0:T(8,128)(2,1)S(1)} %reshape.186, bf16[16,1024,1,128]{3,1,2,0:T(8,128)(2,1)} %param.28, pred[16,1024]{1,0:T(8,128)(4,1)S(1)} %iota_compare_fusion.1), kind=kOutput, calls=%fused_computation.96 | convolution fusion | flops 17432448 | bytes 5276672 | tf_op jit(solution)/shard_map/skgd,slkd->skgl/dot_general | solution.py:31
  94.5 1.4 fusion.37
  96.0 30.5 %all_gather.6 = bf16[128,512]{1,0:T(8,128)(2,1)S(1)} all-gather(bf16[16,512]{1,0:T(8,128)(2,1)S(1)} %reshape.191), channel_id=1, replica_groups=mesh['ep'=8,'tp'=4] {'ep'}, dimensions={0}, use_global_device_ids=true | all-gather | bytes 147456 | tf_op jit(solution)/shard_map/all_gather | solution.py:104
  126.6 0.9 fusion.85
  127.7 31.3 %all-reduce.2.cloned.1.call-done = f32[8,16,512]{2,1,0:T(8,128)} async-done(((f32[8,16,512]{2,1,0:T(8,128)}), f32[8,16,512]{2,1,0:T(8,128)}) %all-reduce.2.cloned.1.call-update) | async-done | bytes 262160 | tf_op jit(solution)/shard_map/psum | solution.py:108
  159.0 5.5 %all-to-all-start.1 = ((f32[8,16,512]{2,1,0:T(8,128)}), f32[8,16,512]{2,1,0:T(8,128)S(1)}, u32[]{:S(2)}, u32[]{:S(2)}) async-start(f32[8,16,512]{2,1,0:T(8,128)} %all-reduce.2.cloned.1.call-done), calls=%async_computation.2 | async-start | bytes 524288 | tf_op jit(solution)/shard_map/all_to_all | solution.py:109
  165.2 7.6 %all-to-all-done.1 = f32[8,16,512]{2,1,0:T(8,128)S(1)} async-done(((f32[8,16,512]{2,1,0:T(8,128)}), f32[8,16,512]{2,1,0:T(8,128)S(1)}, u32[]{:S(2)}, u32[]{:S(2)}) %all-to-all-start.1) | async-done | bytes 262176 | tf_op jit(solution)/shard_map/all_to_all | solution.py:109
  173.1 1.5 convolution_convert_fusion
  174.6 3.6 %all-to-all-start.2 = ((bf16[8,16,4096]{2,1,0:T(8,128)(2,1)}), bf16[8,16,4096]{2,1,0:T(8,128)(2,1)S(1)}, u32[]{:S(2)}, u32[]{:S(2)}) async-start(bf16[8,16,4096]{2,1,0:T(8,128)(2,1)} %bitcast.112), calls=%async_computation.3 | async-start | bytes 2097152 | tf_op jit(solution)/shard_map/all_to_all | solution.py:132
  178.9 27.4 %all-to-all-done.2 = bf16[8,16,4096]{2,1,0:T(8,128)(2,1)S(1)} async-done(((bf16[8,16,4096]{2,1,0:T(8,128)(2,1)}), bf16[8,16,4096]{2,1,0:T(8,128)(2,1)S(1)}, u32[]{:S(2)}, u32[]{:S(2)}) %all-to-all-start.2) | async-done | bytes 1048608 | tf_op jit(solution)/shard_map/all_to_all | solution.py:132
  206.3 2.0 fusion.10
  208.4 4.3 %fusion.6 = f32[128,4096]{1,0:T(8,128)} fusion(bf16[1,256,4096]{2,1,0:T(8,128)(2,1)S(1)} %copy-done, bf16[128,4096]{1,0:T(8,128)(2,1)S(1)} %bitcast.110, bf16[1,4096,256]{2,1,0:T(8,128)(2,1)} %param.34, f32[128,256]{1,0:T(8,128)S(1)} %fusion.10), kind=kOutput, calls=%fused_computation.8 | convolution fusion | flops 537067520 | bytes 7471104 | tf_op jit(solution)/shard_map/dot_general | solution.py:138
  212.7 14.0 %all-gather.2.cloned.1.call-done = bf16[128,4096]{1,0:T(8,128)(2,1)} async-done(((bf16[16,4096]{1,0:T(8,128)(2,1)}), bf16[128,4096]{1,0:T(8,128)(2,1)}) %all-gather.2.cloned.1.call-update) | async-done | bytes 1048592 | tf_op jit(solution)/shard_map/all_gather | solution.py:150
  226.7 3.3 fusion.86
  230.1 4.3 %fusion.25 = f32[128,1024]{1,0:T(8,128)} fusion(bf16[512,1024]{1,0:T(8,128)(2,1)} %param.40, bf16[128,4096]{1,0:T(8,128)(2,1)S(1)} %copy-done.2, bf16[4096,512]{1,0:T(8,128)(2,1)} %param.39, f32[128,512]{1,0:T(8,128)S(1)} %fusion.86), kind=kOutput, calls=%fused_computation.20 | convolution fusion | flops 671481856 | bytes 7077888 | tf_op jit(solution)/shard_map/dot_general | solution.py:157
  234.6 24.5 %reduce-scatter.6.cloned.1.call-done = f32[128,1024]{1,0:T(8,128)} async-done(((f32[128,4096]{1,0:T(8,128)}), f32[128,1024]{1,0:T(8,128)}) %reduce-scatter.6.cloned.1.call-update) | async-done | bytes 524304 | tf_op jit(solution)/shard_map/reduce_scatter | solution.py:139
  259.0 1.8 convert_element_type.82
  260.8 5.5 %all-to-all-start.3 = ((bf16[8,16,1024]{2,1,0:T(8,128)(2,1)}), bf16[8,16,1024]{2,1,0:T(8,128)(2,1)S(1)}, u32[]{:S(2)}, u32[]{:S(2)}) async-start(bf16[8,16,1024]{2,1,0:T(8,128)(2,1)} %bitcast.19), calls=%async_computation.5 | async-start | bytes 524288 | tf_op jit(solution)/shard_map/all_to_all | solution.py:141
  266.4 0.9 fusion.43
  267.3 8.6 %all-to-all-done.3 = bf16[8,16,1024]{2,1,0:T(8,128)(2,1)S(1)} async-done(((bf16[8,16,1024]{2,1,0:T(8,128)(2,1)}), bf16[8,16,1024]{2,1,0:T(8,128)(2,1)S(1)}, u32[]{:S(2)}, u32[]{:S(2)}) %all-to-all-start.3) | async-done | bytes 262176 | tf_op jit(solution)/shard_map/all_to_all | solution.py:141
  276.9 48.0 %reduce-scatter.8.cloned.1.call-done = f32[16,1024]{1,0:T(8,128)} async-done(((f32[128,1024]{1,0:T(8,128)}), f32[16,1024]{1,0:T(8,128)}) %reduce-scatter.8.cloned.1.call-update) | async-done | bytes 65552 | tf_op jit(solution)/shard_map/reduce_scatter | solution.py:156
  324.9 1.5 add_convert_fusion
  (73 shorter events, 5.7 us)
Async XLA Ops:
  6.5 201.8 %copy-start = (bf16[1,256,4096]{2,1,0:T(8,128)(2,1)S(1)}, bf16[1,256,4096]{2,1,0:T(8,128)(2,1)}, u32[]{:S(2)}) copy-start(bf16[1,256,4096]{2,1,0:T(8,128)(2,1)} %param.35) | copy-start | bytes 6291460
  6.5 22.8 %copy-start.12 = (s32[16]{0:T(128)S(1)}, s32[16]{0:T(128)}, u32[]{:S(2)}) copy-start(s32[16]{0:T(128)} %param.30) | copy-start | bytes 196
  6.5 22.6 %copy-start.3 = (f32[16,1024,8]{1,2,0:T(8,128)S(1)}, f32[16,1024,8]{1,2,0:T(8,128)}, u32[]{:S(2)}) copy-start(f32[16,1024,8]{1,2,0:T(8,128)} %param.29) | copy-start | bytes 1572868
  6.5 83.1 %copy-start.13 = (f32[8]{0:T(128)S(1)}, f32[8]{0:T(128)}, u32[]{:S(2)}) copy-start(f32[8]{0:T(128)} %param.27) | copy-start | bytes 100
  6.5 82.0 %reduce-scatter.4.cloned.1.call-start = ((), (), s32[]{:S(2)}) async-start(), calls=%async_computation.7 | async-start | bytes 442368 | tf_op jit(solution)/shard_map/reduce_scatter | solution.py:86
  28.3 130.7 %all-reduce.2.cloned.1.call-start = ((), (), s32[]{:S(2)}) async-start(), calls=%async_computation.8 | async-start | bytes 524288 | tf_op jit(solution)/shard_map/psum | solution.py:108
  89.5 5.0 %copy-start.1 = (bf16[16,1024,1,128]{3,1,2,0:T(8,128)(2,1)S(1)}, bf16[16,1024,1,128]{3,1,2,0:T(8,128)(2,1)}, u32[]{:S(2)}) copy-start(bf16[16,1024,1,128]{3,1,2,0:T(8,128)(2,1)} %param.28) | copy-start | bytes 12582916
  94.2 32.3 %copy-start.8 = (bf16[512,512]{1,0:T(8,128)(2,1)S(1)}, bf16[512,512]{1,0:T(8,128)(2,1)}, u32[]{:S(2)}) copy-start(bf16[512,512]{1,0:T(8,128)(2,1)} %param.31) | copy-start | bytes 1572868
  94.2 33.3 %copy-start.10 = (s32[16,4]{0,1:T(4,128)S(1)}, s32[16,4]{0,1:T(4,128)}, u32[]{:S(2)}) copy-start(s32[16,4]{0,1:T(4,128)} %param.36) | copy-start | bytes 772
  94.5 78.3 %copy-start.4 = (bf16[16,4096]{1,0:T(8,128)(2,1)S(1)}, bf16[16,4096]{1,0:T(8,128)(2,1)}, u32[]{:S(2)}) copy-start(bf16[16,4096]{1,0:T(8,128)(2,1)} %param.21) | copy-start | bytes 393220
  94.5 78.5 %copy-start.9 = (f32[4096]{0:T(1024)S(1)}, f32[4096]{0:T(1024)}, u32[]{:S(2)}) copy-start(f32[4096]{0:T(1024)} %param.32) | copy-start | bytes 49156
  159.0 13.7 %all-to-all-start.1 = ((f32[8,16,512]{2,1,0:T(8,128)}), f32[8,16,512]{2,1,0:T(8,128)S(1)}, u32[]{:S(2)}, u32[]{:S(2)}) async-start(f32[8,16,512]{2,1,0:T(8,128)} %all-reduce.2.cloned.1.call-done), calls=%async_computation.2 | async-start | bytes 524288 | tf_op jit(solution)/shard_map/all_to_all | solution.py:109
  173.0 1.6 copy-start.7
  173.1 5.1 %copy-start.5 = (bf16[16,4096]{1,0:T(8,128)(2,1)}, bf16[16,4096]{1,0:T(8,128)(2,1)S(1)}, u32[]{:S(2)}) copy-start(bf16[16,4096]{1,0:T(8,128)(2,1)S(1)} %fusion.47) | copy-start | bytes 393220
  174.6 31.8 %all-to-all-start.2 = ((bf16[8,16,4096]{2,1,0:T(8,128)(2,1)}), bf16[8,16,4096]{2,1,0:T(8,128)(2,1)S(1)}, u32[]{:S(2)}, u32[]{:S(2)}) async-start(bf16[8,16,4096]{2,1,0:T(8,128)(2,1)} %bitcast.112), calls=%async_computation.3 | async-start | bytes 2097152 | tf_op jit(solution)/shard_map/all_to_all | solution.py:132
  178.1 48.6 %all-gather.2.cloned.1.call-start = ((), (), s32[]{:S(2)}) async-start(), calls=%async_computation.10 | async-start | bytes 1179648 | tf_op jit(solution)/shard_map/all_gather | solution.py:150
  178.9 80.2 %reduce-scatter.6.cloned.1.call-start = ((), (), s32[]{:S(2)}) async-start(), calls=%async_computation.9 | async-start | bytes 2621440 | tf_op jit(solution)/shard_map/reduce_scatter | solution.py:139
  212.7 112.2 %reduce-scatter.8.cloned.1.call-start = ((), (), s32[]{:S(2)}) async-start(), calls=%async_computation.11 | async-start | bytes 589824 | tf_op jit(solution)/shard_map/reduce_scatter | solution.py:156
  226.7 3.3 copy-start.2
  230.1 4.3 %copy-start.11 = (f32[16,4]{0,1:T(4,128)S(1)}, f32[16,4]{0,1:T(4,128)}, u32[]{:S(2)}) copy-start(f32[16,4]{0,1:T(4,128)} %param.37) | copy-start | bytes 772
  230.1 36.3 %copy-start.6 = (bf16[16,4096]{1,0:T(8,128)(2,1)S(1)}, bf16[16,4096]{1,0:T(8,128)(2,1)}, u32[]{:S(2)}) copy-start(bf16[16,4096]{1,0:T(8,128)(2,1)} %copy-done.5) | copy-start | bytes 393220
  260.8 15.1 %all-to-all-start.3 = ((bf16[8,16,1024]{2,1,0:T(8,128)(2,1)}), bf16[8,16,1024]{2,1,0:T(8,128)(2,1)S(1)}, u32[]{:S(2)}, u32[]{:S(2)}) async-start(bf16[8,16,1024]{2,1,0:T(8,128)(2,1)} %bitcast.19), calls=%async_computation.5 | async-start | bytes 524288 | tf_op jit(solution)/shard_map/all_to_all | solution.py:141
Sparse Core Ops, SparseCore 0:
  28.5 60.0 reduce-scatter.3
  127.6 31.3 all-reduce.1
  181.1 45.6 all-gather.1
  229.1 29.8 reduce-scatter.5
  262.2 62.6 reduce-scatter.7
where the time goes:
time: 334 us; the launch traced here: 333 us
  waiting for transfers between devices  221 us (66%)
  blocking collectives  44.9 us (13%)
  matrix products  26.6 us (8%)
  starting transfers between devices  14.8 us (4%)
  between operations  13.5 us (4%)
  other arithmetic  10.4 us (3%)
    reduce_scatter x1, waiting for transfers between devices, shards(): lax.psum_scatter(jnp.concatenate([jnp.dot(row_block, matrix, preferred_el...  59.1 us
    reduce_scatter x1, waiting for transfers between devices, shards(): lax.psum_scatter(jnp.dot(row_block, dense_down, preferred_element_type=jn...  48 us
    psum x1, waiting for transfers between devices, shards(): column_total = lax.psum(column_terms, 'tp')  31.3 us
    all_gather x1, blocking collectives, shards(): lax.all_gather(attended, 'ep', axis=0, tiled=True)  30.5 us
    all_to_all x1, waiting for transfers between devices, shards(): lax.all_to_all(outgoing, 'ep', split_axis=0, concat_axis=0, tiled=True)  27.4 us
    reduce_scatter x1, waiting for transfers between devices, shards(): lax.psum_scatter(partial_rows, 'tp', scatter_dimension=1, tiled=True)  24.5 us
    all_to_all x1, blocking collectives, shards(): lax.all_to_all(normed, 'ep', split_axis=1, concat_axis=0, tiled=True)  14.4 us
    all_gather x1, waiting for transfers between devices, shards(): piece = lax.all_gather(second, 'ep', axis=0, tiled=True)  14 us
  transfers between devices with their start and end apart: 8, of which 8 were waited for; matrix products, arithmetic and copies ran while one was open for 6% of the time, Pallas kernels for 0%

commit v1 on v0

--- a/solution.py
+++ b/solution.py
@@ -4,6 +4,15 @@
 from jax.sharding import PartitionSpec as P
 
 EPS = 1e-06
+
+
+def put_the_orders(state):
+    width = lax.axis_size("tp")
+    r2 = state
+    for it in [[(d, d ^ q) for d in range(width)] for q in (1, 2, 4, 8, 16) if q < width]:
+        built = lax.ppermute(r2, "tp", it)
+        r2 = r2 + built
+    return r2
 
 
 def rms_scaled(matrix, gains):
@@ -105,7 +114,7 @@
         out_weight,
         preferred_element_type=jnp.float32,
     )
-    column_total = lax.psum(column_terms, "tp")
+    column_total = put_the_orders(column_terms)
     summed = lax.all_to_all(column_total, "ep", split_axis=0, concat_axis=1, tiled=True)
     mixed = (tokens.astype(jnp.float32) + summed).astype(jnp.bfloat16)
     second = rms_scaled(mixed, mix_gain).astype(jnp.bfloat16)

time: 334 us -> 312 us (0.934)
  waiting for transfers between devices: 221 us -> 199 us
    psum x1 -> x0, waiting for transfers between devices: 31.3 us -> none  [shards(): column_total = lax.psum(column_terms, 'tp')]
    ppermute x0 -> x2, waiting for transfers between devices: none -> 8.23 us  [put_the_orders(): built = lax.ppermute(r2, 'tp', it)]
  transfers between devices with their start and end apart: 8 -> 9, of which waited for: 8 -> 9; matrix products, arithmetic and copies ran while one was open for 6% -> 6% of each run, Pallas kernels for 0% -> 0%
where the time goes in v1:
time: 312 us; the launch traced here: 311 us
  waiting for transfers between devices  199 us (64%)
  blocking collectives  44.9 us (14%)
  matrix products  25.9 us (8%)
  starting transfers between devices  14.5 us (5%)
  between operations  13.4 us (4%)
  other arithmetic  11.2 us (4%)
    reduce_scatter x1, waiting for transfers between devices, shards(): lax.psum_scatter(jnp.concatenate([jnp.dot(row_block, matrix, preferred_el...  59.2 us
    reduce_scatter x1, waiting for transfers between devices, shards(): lax.psum_scatter(jnp.dot(row_block, dense_down, preferred_element_type=jn...  48 us
    all_gather x1, blocking collectives, shards(): lax.all_gather(attended, 'ep', axis=0, tiled=True)  30.5 us
    all_to_all x1, waiting for transfers between devices, shards(): lax.all_to_all(outgoing, 'ep', split_axis=0, concat_axis=0, tiled=True)  28.8 us
    reduce_scatter x1, waiting for transfers between devices, shards(): lax.psum_scatter(partial_rows, 'tp', scatter_dimension=1, tiled=True)  24.6 us
    all_to_all x1, blocking collectives, shards(): lax.all_to_all(normed, 'ep', split_axis=1, concat_axis=0, tiled=True)  14.4 us
    all_gather x1, waiting for transfers between devices, shards(): piece = lax.all_gather(second, 'ep', axis=0, tiled=True)  13.3 us
    all_to_all x1, waiting for transfers between devices, shards(): lax.all_to_all(replies, 'ep', split_axis=0, concat_axis=0, tiled=True)  8.57 us
  transfers between devices with their start and end apart: 9, of which 9 were waited for; matrix products, arithmetic and copies ran while one was open for 6% of the time, Pallas kernels for 0%

profile of v1, /device:TPU:0, one launch (start us, length us, event | category | flops | bytes accessed | tf_op | source)
XLA Modules:
  0.0 310.9 jit_solution(5733466003041281708)
XLA Ops:
  6.6 1.2 fusion.48
  7.8 1.0 fusion.50
  8.9 14.4 %all_to_all.48 = bf16[16,8,512]{2,0,1:T(8,128)(2,1)S(1)} all-to-all(bf16[16,8,512]{2,0,1:T(8,128)(2,1)S(1)} %bitcast.120), channel_id=1, replica_groups=mesh['ep'=8,'tp'=4] {'ep'}, dimensions={1} | all-to-all | bytes 262144 | tf_op jit(solution)/shard_map/all_to_all | solution.py:93
  24.1 1.0 fusion.83
  25.2 1.0 fusion.82
  26.2 1.3 fusion.81
  27.5 0.9 pad_maximum_fusion
  29.4 59.2 %reduce-scatter.4.cloned.1.call-done = f32[16,648]{1,0:T(8,128)} async-done(((f32[128,648]{1,0:T(8,128)}), f32[16,648]{1,0:T(8,128)}) %reduce-scatter.4.cloned.1.call-update) | async-done | bytes 41488 | tf_op jit(solution)/shard_map/reduce_scatter | solution.py:95
  89.7 0.9 fusion.69
  90.5 3.7 %fusion.80 = (f32[16,8]{1,0:T(8,128)S(1)}, f32[16,1,8,1024]{3,2,0,1:T(8,128)S(1)}) fusion(f32[16,1024,8]{1,2,0:T(8,128)S(1)} %copy-done.3, f32[16,8]{1,0:T(8,128)S(1)} %fusion.69, bf16[16,8,64]{2,1,0:T(8,128)(2,1)S(1)} %reshape.186, bf16[16,1024,1,128]{3,1,2,0:T(8,128)(2,1)} %param.28, pred[16,1024]{1,0:T(8,128)(4,1)S(1)} %iota_compare_fusion.1), kind=kOutput, calls=%fused_computation.96 | convolution fusion | flops 17432448 | bytes 5276672 | tf_op jit(solution)/shard_map/skgd,slkd->skgl/dot_general | solution.py:40
  94.6 1.4 fusion.37
  96.1 30.5 %all_gather.6 = bf16[128,512]{1,0:T(8,128)(2,1)S(1)} all-gather(bf16[16,512]{1,0:T(8,128)(2,1)S(1)} %reshape.191), channel_id=1, replica_groups=mesh['ep'=8,'tp'=4] {'ep'}, dimensions={0}, use_global_device_ids=true | all-gather | bytes 147456 | tf_op jit(solution)/shard_map/all_gather | solution.py:113
  126.9 1.5 collective-permute-done
  128.5 1.5 collective-permute-start.1
  130.2 6.7 %collective-permute-done.1 = f32[128,512]{1,0:T(8,128)S(1)} collective-permute-done((f32[128,512]{1,0:T(8,128)S(1)}, f32[128,512]{1,0:T(8,128)S(1)}, u32[]{:S(2)}, u32[]{:S(2)}) %collective-permute-start.1) | collective-permute-done | bytes 262176 | tf_op jit(solution)/shard_map/ppermute | solution.py:13
  137.6 3.7 %all-to-all-start.1 = ((f32[8,16,512]{2,1,0:T(8,128)}), f32[8,16,512]{2,1,0:T(8,128)S(1)}, u32[]{:S(2)}, u32[]{:S(2)}) async-start(f32[8,16,512]{2,1,0:T(8,128)} %bitcast.12), calls=%async_computation.2 | async-start | bytes 524288 | tf_op jit(solution)/shard_map/all_to_all | solution.py:118
  141.9 7.9 %all-to-all-done.1 = f32[8,16,512]{2,1,0:T(8,128)S(1)} async-done(((f32[8,16,512]{2,1,0:T(8,128)}), f32[8,16,512]{2,1,0:T(8,128)S(1)}, u32[]{:S(2)}, u32[]{:S(2)}) %all-to-all-start.1) | async-done | bytes 262176 | tf_op jit(solution)/shard_map/all_to_all | solution.py:118
  150.1 1.5 convolution_convert_fusion
  151.6 3.6 %all-to-all-start.2 = ((bf16[8,16,4096]{2,1,0:T(8,128)(2,1)}), bf16[8,16,4096]{2,1,0:T(8,128)(2,1)S(1)}, u32[]{:S(2)}, u32[]{:S(2)}) async-start(bf16[8,16,4096]{2,1,0:T(8,128)(2,1)} %bitcast.112), calls=%async_computation.3 | async-start | bytes 2097152 | tf_op jit(solution)/shard_map/all_to_all | solution.py:141
  155.9 28.8 %all-to-all-done.2 = bf16[8,16,4096]{2,1,0:T(8,128)(2,1)S(1)} async-done(((bf16[8,16,4096]{2,1,0:T(8,128)(2,1)}), bf16[8,16,4096]{2,1,0:T(8,128)(2,1)S(1)}, u32[]{:S(2)}, u32[]{:S(2)}) %all-to-all-start.2) | async-done | bytes 1048608 | tf_op jit(solution)/shard_map/all_to_all | solution.py:141
  184.8 2.0 fusion.10
  186.8 4.2 %fusion.6 = f32[128,4096]{1,0:T(8,128)} fusion(bf16[1,256,4096]{2,1,0:T(8,128)(2,1)S(1)} %copy-done, bf16[128,4096]{1,0:T(8,128)(2,1)S(1)} %bitcast.110, bf16[1,4096,256]{2,1,0:T(8,128)(2,1)} %param.34, f32[128,256]{1,0:T(8,128)S(1)} %fusion.10), kind=kOutput, calls=%fused_computation.8 | convolution fusion | flops 537067520 | bytes 7471104 | tf_op jit(solution)/shard_map/dot_general | solution.py:147
  191.1 13.3 %all-gather.2.cloned.1.call-done = bf16[128,4096]{1,0:T(8,128)(2,1)} async-done(((bf16[16,4096]{1,0:T(8,128)(2,1)}), bf16[128,4096]{1,0:T(8,128)(2,1)}) %all-gather.2.cloned.1.call-update) | async-done | bytes 1048592 | tf_op jit(solution)/shard_map/all_gather | solution.py:159
  204.5 3.3 %fusion.86 = f32[128,512]{1,0:T(8,128)S(1)} fusion(bf16[128,4096]{1,0:T(8,128)(2,1)} %all-gather.2.cloned.1.call-done, bf16[4096,512]{1,0:T(8,128)(2,1)} %param.38), kind=kOutput, calls=%fused_computation.102 | convolution fusion | flops 536870912 | bytes 5505024 | tf_op jit(solution)/shard_map/dot_general | solution.py:161
  207.8 4.3 %fusion.25 = f32[128,1024]{1,0:T(8,128)} fusion(bf16[512,1024]{1,0:T(8,128)(2,1)} %param.40, bf16[128,4096]{1,0:T(8,128)(2,1)S(1)} %copy-done.2, bf16[4096,512]{1,0:T(8,128)(2,1)} %param.39, f32[128,512]{1,0:T(8,128)S(1)} %fusion.86), kind=kOutput, calls=%fused_computation.20 | convolution fusion | flops 671481856 | bytes 7077888 | tf_op jit(solution)/shard_map/dot_general | solution.py:166
  212.3 24.6 %reduce-scatter.6.cloned.1.call-done = f32[128,1024]{1,0:T(8,128)} async-done(((f32[128,4096]{1,0:T(8,128)}), f32[128,1024]{1,0:T(8,128)}) %reduce-scatter.6.cloned.1.call-update) | async-done | bytes 524304 | tf_op jit(solution)/shard_map/reduce_scatter | solution.py:148
  236.9 1.8 convert_element_type.82
  238.7 5.5 %all-to-all-start.3 = ((bf16[8,16,1024]{2,1,0:T(8,128)(2,1)}), bf16[8,16,1024]{2,1,0:T(8,128)(2,1)S(1)}, u32[]{:S(2)}, u32[]{:S(2)}) async-start(bf16[8,16,1024]{2,1,0:T(8,128)(2,1)} %bitcast.19), calls=%async_computation.5 | async-start | bytes 524288 | tf_op jit(solution)/shard_map/all_to_all | solution.py:150
  244.3 0.9 fusion.43
  245.2 8.6 %all-to-all-done.3 = bf16[8,16,1024]{2,1,0:T(8,128)(2,1)S(1)} async-done(((bf16[8,16,1024]{2,1,0:T(8,128)(2,1)}), bf16[8,16,1024]{2,1,0:T(8,128)(2,1)S(1)}, u32[]{:S(2)}, u32[]{:S(2)}) %all-to-all-start.3) | async-done | bytes 262176 | tf_op jit(solution)/shard_map/all_to_all | solution.py:150
  254.8 48.0 %reduce-scatter.8.cloned.1.call-done = f32[16,1024]{1,0:T(8,128)} async-done(((f32[128,1024]{1,0:T(8,128)}), f32[16,1024]{1,0:T(8,128)}) %reduce-scatter.8.cloned.1.call-update) | async-done | bytes 65552 | tf_op jit(solution)/shard_map/reduce_scatter | solution.py:165
  302.8 1.5 add_convert_fusion
  (76 shorter events, 7.6 us)
Async XLA Ops:
  6.5 180.3 %copy-start = (bf16[1,256,4096]{2,1,0:T(8,128)(2,1)S(1)}, bf16[1,256,4096]{2,1,0:T(8,128)(2,1)}, u32[]{:S(2)}) copy-start(bf16[1,256,4096]{2,1,0:T(8,128)(2,1)} %param.35) | copy-start | bytes 6291460
  6.5 22.7 %copy-start.12 = (s32[16]{0:T(128)S(1)}, s32[16]{0:T(128)}, u32[]{:S(2)}) copy-start(s32[16]{0:T(128)} %param.30) | copy-start | bytes 196
  6.5 22.6 %copy-start.3 = (f32[16,1024,8]{1,2,0:T(8,128)S(1)}, f32[16,1024,8]{1,2,0:T(8,128)}, u32[]{:S(2)}) copy-start(f32[16,1024,8]{1,2,0:T(8,128)} %param.29) | copy-start | bytes 1572868
  6.5 83.1 %copy-start.13 = (f32[8]{0:T(128)S(1)}, f32[8]{0:T(128)}, u32[]{:S(2)}) copy-start(f32[8]{0:T(128)} %param.27) | copy-start | bytes 100
  6.5 82.0 %reduce-scatter.4.cloned.1.call-start = ((), (), s32[]{:S(2)}) async-start(), calls=%async_computation.7 | async-start | bytes 442368 | tf_op jit(solution)/shard_map/reduce_scatter | solution.py:95
  89.5 5.0 %copy-start.1 = (bf16[16,1024,1,128]{3,1,2,0:T(8,128)(2,1)S(1)}, bf16[16,1024,1,128]{3,1,2,0:T(8,128)(2,1)}, u32[]{:S(2)}) copy-start(bf16[16,1024,1,128]{3,1,2,0:T(8,128)(2,1)} %param.28) | copy-start | bytes 12582916
  94.2 32.3 %copy-start.8 = (bf16[512,512]{1,0:T(8,128)(2,1)S(1)}, bf16[512,512]{1,0:T(8,128)(2,1)}, u32[]{:S(2)}) copy-start(bf16[512,512]{1,0:T(8,128)(2,1)} %param.31) | copy-start | bytes 1572868
  94.5 35.5 %copy-start.10 = (s32[16,4]{0,1:T(4,128)S(1)}, s32[16,4]{0,1:T(4,128)}, u32[]{:S(2)}) copy-start(s32[16,4]{0,1:T(4,128)} %param.36) | copy-start | bytes 772
  94.5 55.3 %copy-start.4 = (bf16[16,4096]{1,0:T(8,128)(2,1)S(1)}, bf16[16,4096]{1,0:T(8,128)(2,1)}, u32[]{:S(2)}) copy-start(bf16[16,4096]{1,0:T(8,128)(2,1)} %param.21) | copy-start | bytes 393220
  94.5 55.5 %copy-start.9 = (f32[4096]{0:T(1024)S(1)}, f32[4096]{0:T(1024)}, u32[]{:S(2)}) copy-start(f32[4096]{0:T(1024)} %param.32) | copy-start | bytes 49156
  126.8 1.6 collective-permute-start
  128.5 8.4 %collective-permute-start.1 = (f32[128,512]{1,0:T(8,128)S(1)}, f32[128,512]{1,0:T(8,128)S(1)}, u32[]{:S(2)}, u32[]{:S(2)}) collective-permute-start(f32[128,512]{1,0:T(8,128)S(1)} %add.115), channel_id=1, source_target_pairs={{0,2},{1,3},{2,0},{3,1},{4,6},{5,7},{6,4},{7,5},{8,10},{9,11},{10,... | collective-permute-start | bytes 786440 | tf_op jit(solution)/shard_map/ppermute | solution.py:13
  137.6 12.2 %all-to-all-start.1 = ((f32[8,16,512]{2,1,0:T(8,128)}), f32[8,16,512]{2,1,0:T(8,128)S(1)}, u32[]{:S(2)}, u32[]{:S(2)}) async-start(f32[8,16,512]{2,1,0:T(8,128)} %bitcast.12), calls=%async_computation.2 | async-start | bytes 524288 | tf_op jit(solution)/shard_map/all_to_all | solution.py:118
  150.0 1.6 copy-start.7
  150.1 5.1 %copy-start.5 = (bf16[16,4096]{1,0:T(8,128)(2,1)}, bf16[16,4096]{1,0:T(8,128)(2,1)S(1)}, u32[]{:S(2)}) copy-start(bf16[16,4096]{1,0:T(8,128)(2,1)S(1)} %fusion.47) | copy-start | bytes 393220
  151.6 33.2 %all-to-all-start.2 = ((bf16[8,16,4096]{2,1,0:T(8,128)(2,1)}), bf16[8,16,4096]{2,1,0:T(8,128)(2,1)S(1)}, u32[]{:S(2)}, u32[]{:S(2)}) async-start(bf16[8,16,4096]{2,1,0:T(8,128)(2,1)} %bitcast.112), calls=%async_computation.3 | async-start | bytes 2097152 | tf_op jit(solution)/shard_map/all_to_all | solution.py:141
  155.1 49.3 %all-gather.2.cloned.1.call-start = ((), (), s32[]{:S(2)}) async-start(), calls=%async_computation.9 | async-start | bytes 1179648 | tf_op jit(solution)/shard_map/all_gather | solution.py:159
  155.9 81.0 %reduce-scatter.6.cloned.1.call-start = ((), (), s32[]{:S(2)}) async-start(), calls=%async_computation.8 | async-start | bytes 2621440 | tf_op jit(solution)/shard_map/reduce_scatter | solution.py:148
  191.1 111.7 %reduce-scatter.8.cloned.1.call-start = ((), (), s32[]{:S(2)}) async-start(), calls=%async_computation.10 | async-start | bytes 589824 | tf_op jit(solution)/shard_map/reduce_scatter | solution.py:165
  204.5 3.3 %copy-start.2 = (bf16[128,4096]{1,0:T(8,128)(2,1)S(1)}, bf16[128,4096]{1,0:T(8,128)(2,1)}, u32[]{:S(2)}) copy-start(bf16[128,4096]{1,0:T(8,128)(2,1)} %all-gather.2.cloned.1.call-done) | copy-start | bytes 3145732
  207.8 4.3 %copy-start.11 = (f32[16,4]{0,1:T(4,128)S(1)}, f32[16,4]{0,1:T(4,128)}, u32[]{:S(2)}) copy-start(f32[16,4]{0,1:T(4,128)} %param.37) | copy-start | bytes 772
  207.8 36.4 %copy-start.6 = (bf16[16,4096]{1,0:T(8,128)(2,1)S(1)}, bf16[16,4096]{1,0:T(8,128)(2,1)}, u32[]{:S(2)}) copy-start(bf16[16,4096]{1,0:T(8,128)(2,1)} %copy-done.5) | copy-start | bytes 393220
  238.7 15.1 %all-to-all-start.3 = ((bf16[8,16,1024]{2,1,0:T(8,128)(2,1)}), bf16[8,16,1024]{2,1,0:T(8,128)(2,1)S(1)}, u32[]{:S(2)}, u32[]{:S(2)}) async-start(bf16[8,16,1024]{2,1,0:T(8,128)(2,1)} %bitcast.19), calls=%async_computation.5 | async-start | bytes 524288 | tf_op jit(solution)/shard_map/all_to_all | solution.py:150
Sparse Core Ops, SparseCore 0:
  28.5 60.0 reduce-scatter.3
  158.1 46.3 all-gather.1
  207.0 29.8 reduce-scatter.5
  240.1 62.6 reduce-scatter.7
